TPU v7x, 32 devices: a whole 2x2x4 slice. The times are simulated.
32 devices in a mesh: kv: 8 (over z, y), tp: 4 (over x, core).
Axes of the slice: x: 2, y: 2, z: 4, core: 2. Of those that a mesh axis runs over, the one named last changes fastest.
Arguments:
- stream: bfloat16 [24, 4096], P(None, ('kv', 'tp')), may hold values from -50 to 50
- attention_gain: float32 [4096], P(('kv', 'tp')), may hold values from 0.1 to 1.9
- query_down: bfloat16 [4096, 1536], P(('kv', 'tp')), may hold values from -0.09375 to 0.09375
- latent_down: bfloat16 [4096, 512], P(('kv', 'tp')), may hold values from -0.09375 to 0.09375
- rotary_down: bfloat16 [4096, 64], P(('kv', 'tp')), may hold values from -0.1875 to 0.1875
- query_gain: float32 [1536], replicated, may hold values from 0.1 to 1.9
- latent_gain: float32 [512], replicated, may hold values from 0.1 to 1.9
- query_content: bfloat16 [1536, 2048], P(None, 'tp'), may hold values from -0.15625 to 0.15625
- query_rotary: bfloat16 [1536, 1024], P(None, 'tp'), may hold values from -0.15625 to 0.15625
- key_absorb: bfloat16 [16, 128, 512], P('tp'), may hold values from -0.5 to 0.5
- value_absorb: bfloat16 [16, 512, 128], P('tp'), may hold values from -0.25 to 0.25
- latent_cache: bfloat16 [24, 2048, 512], P(None, 'kv'), may hold values from -1200 to 1200
- rotary_cache: bfloat16 [24, 2048, 64], P(None, 'kv'), may hold values from -5 to 5
- head_gain: float32 [2048], P('tp'), may hold values from 0.1 to 1.9
- output_weight: bfloat16 [2048, 4096], P('tp', 'kv'), may hold values from -0.125 to 0.125
- mixer_gain: float32 [4096], P('kv'), may hold values from 0.1 to 1.9
- gate_weight: bfloat16 [4096, 11264], P('kv', 'tp'), may hold values from -0.09375 to 0.09375
- up_weight: bfloat16 [4096, 11264], P('kv', 'tp'), may hold values from -0.09375 to 0.09375
- down_weight: bfloat16 [11264, 4096], P('tp', 'kv'), may hold values from -0.0546875 to 0.0546875
Outputs:
- stream_out: bfloat16 [24, 4096], P(None, ('kv', 'tp'))
All inputs are finite; a program needn't handle non-finite values.
Results may differ from a plain program's by a relative error of at most 0.018.
Values may be sent and summed in bfloat16 or wider, within the bound.
A program may use at most 64 MiB of HBM per device.

v0:
```python
import jax
import jax.numpy as jnp
from jax import lax
from jax.sharding import PartitionSpec as P

epsilon = 1e-06
rope_base = 10000.0


def rotate(values, position):
    half = values.shape[-1] // 2
    freqs = rope_base ** (-jnp.arange(half, dtype=jnp.float32) * 2.0 / values.shape[-1])
    angle = position * freqs
    cosine = jnp.cos(angle)
    sine = jnp.sin(angle)
    first = values[..., :half]
    second = values[..., half:]
    return jnp.concatenate(
        [first * cosine - second * sine, second * cosine + first * sine], axis=-1
    )


def inv_rms(values):
    return lax.rsqrt(jnp.mean(values * values, axis=-1) + epsilon)


def sum_squares(values):
    return jnp.sum(values * values, axis=-1)


def matmul(left, right):
    return jnp.dot(left, right, preferred_element_type=jnp.float32)


def local(
    stream,
    attention_gain,
    query_down,
    latent_down,
    rotary_down,
    query_gain,
    latent_gain,
    query_content,
    query_rotary,
    key_absorb,
    value_absorb,
    latent_cache,
    rotary_cache,
    head_gain,
    output_weight,
    mixer_gain,
    gate_weight,
    up_weight,
    down_weight,
):
    kv_count = lax.axis_size("kv")
    tp_count = lax.axis_size("tp")
    batch_rows = stream.shape[0]
    model_width = stream.shape[1] * kv_count * tp_count
    position = jnp.float32(latent_cache.shape[1] * kv_count)
    stream_block = lax.all_gather(stream, "tp", axis=1, tiled=True)
    stream_f = stream.astype(jnp.float32)
    first_scaled = (stream_f * attention_gain).astype(jnp.bfloat16)
    query_sum, latent_sum, rotary_sum, square_sum = lax.psum(
        (
            matmul(first_scaled, query_down),
            matmul(first_scaled, latent_down),
            matmul(first_scaled, rotary_down),
            sum_squares(stream_f),
        ),
        ("kv", "tp"),
    )
    first_scale = lax.rsqrt(square_sum / model_width + epsilon)[:, None]
    query_low = first_scale * query_sum
    latent_new = first_scale * latent_sum
    rotary_new = first_scale * rotary_sum
    query_normed = (query_low * inv_rms(query_low)[:, None] * query_gain).astype(jnp.bfloat16)
    latent_row = (latent_new * inv_rms(latent_new)[:, None] * latent_gain).astype(jnp.bfloat16)
    rotary_row = rotate(rotary_new, position).astype(jnp.bfloat16)
    heads_here = key_absorb.shape[0]
    query_plain = matmul(query_normed, query_content).astype(jnp.bfloat16)
    query_plain = query_plain.reshape(batch_rows, heads_here, key_absorb.shape[1])
    query_turned = matmul(query_normed, query_rotary).reshape(
        batch_rows, heads_here, rotary_cache.shape[2]
    )
    query_turned = rotate(query_turned, position).astype(jnp.bfloat16)
    query_latent = jnp.einsum(
        "bhn,hnc->bhc", query_plain, key_absorb, preferred_element_type=jnp.float32
    ).astype(jnp.bfloat16)
    scale = (key_absorb.shape[1] + rotary_cache.shape[2]) ** (-0.5)
    scores = (
        jnp.einsum("bhc,bpc->bhp", query_latent, latent_cache, preferred_element_type=jnp.float32)
        + jnp.einsum("bhr,bpr->bhp", query_turned, rotary_cache, preferred_element_type=jnp.float32)
    ) * scale
    maxima = jnp.max(scores, axis=-1)
    expo = jnp.exp(scores - maxima[..., None])
    totals = jnp.sum(expo, axis=-1)
    weighted = jnp.einsum(
        "bhp,bpc->bhc", expo.astype(jnp.bfloat16), latent_cache, preferred_element_type=jnp.float32
    ).astype(jnp.bfloat16)
    all_maxima, all_totals = (
        lax.all_gather(maxima[None], "kv", axis=0, tiled=True),
        lax.all_gather(totals[None], "kv", axis=0, tiled=True),
    )
    own_score = (
        jnp.sum(
            query_latent.astype(jnp.float32) * latent_row.astype(jnp.float32)[:, None, :], axis=-1
        )
        + jnp.sum(
            query_turned.astype(jnp.float32) * rotary_row.astype(jnp.float32)[:, None, :], axis=-1
        )
    ) * scale
    largest = jnp.maximum(jnp.max(all_maxima, axis=0), own_score)
    factors = jnp.exp(all_maxima - largest[None])
    own_weight = jnp.exp(own_score - largest)
    denominator = jnp.sum(factors * all_totals, axis=0) + own_weight
    merged = jnp.sum(
        factors[..., None]
        * lax.all_gather(weighted[None], "kv", axis=0, tiled=True).astype(jnp.float32),
        axis=0,
    )
    merged = merged + own_weight[..., None] * latent_row.astype(jnp.float32)[:, None, :]
    latent_mix = (merged / denominator[..., None]).astype(jnp.bfloat16)
    head_values = jnp.einsum(
        "bhc,hcv->bhv", latent_mix, value_absorb, preferred_element_type=jnp.float32
    ).astype(jnp.bfloat16)
    head_f = head_values.reshape(batch_rows, heads_here * value_absorb.shape[2]).astype(jnp.float32)
    head_square = lax.psum(sum_squares(head_f), "tp")
    head_scale = lax.rsqrt(head_square / (head_f.shape[1] * tp_count) + epsilon)[:, None]
    head_scaled = (head_f * head_gain).astype(jnp.bfloat16)
    attended = lax.psum(matmul(head_scaled, output_weight).astype(jnp.bfloat16), "tp").astype(
        jnp.float32
    )
    middle = (stream_block.astype(jnp.float32) + head_scale * attended).astype(jnp.bfloat16)
    middle_f = middle.astype(jnp.float32)
    second_scaled = (middle_f * mixer_gain).astype(jnp.bfloat16)
    gate_part = matmul(second_scaled, gate_weight)
    up_part = matmul(second_scaled, up_weight)
    gate_total, up_total, middle_square = (
        lax.psum(gate_part.astype(jnp.bfloat16), "kv").astype(jnp.float32),
        lax.psum(up_part.astype(jnp.bfloat16), "kv").astype(jnp.float32),
        lax.psum(sum_squares(middle_f).astype(jnp.bfloat16), "kv").astype(jnp.float32),
    )
    second_scale = lax.rsqrt(middle_square / model_width + epsilon)[:, None]
    hidden = (jax.nn.silu(second_scale * gate_total) * (second_scale * up_total)).astype(
        jnp.bfloat16
    )
    mixed = lax.psum_scatter(
        matmul(hidden, down_weight).astype(jnp.bfloat16), "tp", scatter_dimension=1, tiled=True
    ).astype(jnp.float32)
    share_width = mixed.shape[1]
    own_middle = lax.dynamic_slice_in_dim(
        middle_f, lax.axis_index("tp") * share_width, share_width, 1
    )
    return (own_middle + mixed).astype(jnp.bfloat16)


def solution(mesh):
    return jax.shard_map(
        local,
        mesh=mesh,
        in_specs=(
            P(None, ("kv", "tp")),
            P(("kv", "tp")),
            P(("kv", "tp"), None),
            P(("kv", "tp"), None),
            P(("kv", "tp"), None),
            P(),
            P(),
            P(None, "tp"),
            P(None, "tp"),
            P("tp", None, None),
            P("tp", None, None),
            P(None, "kv", None),
            P(None, "kv", None),
            P("tp"),
            P("tp", "kv"),
            P("kv"),
            P("kv", "tp"),
            P("kv", "tp"),
            P("tp", "kv"),
        ),
        out_specs=P(None, ("kv", "tp")),
        check_vma=False,
    )
```

profile of v0, /device:TPU:0, one launch (start us, length us, event | category | flops | bytes accessed | tf_op | source)
XLA Modules:
  0.0 365.7 jit_solution(8575871033755606622)
XLA Ops:
  6.5 0.0 copy-start
  6.5 0.0 all-reduce.5.cloned.1.call-start
  6.5 2.0 fusion.32
  8.5 0.0 all-reduce.5.cloned.1.call-update
  8.6 0.0 all-reduce.7.cloned.1.call-start
  8.6 0.8 fusion.26
  9.4 0.6 fusion.35
  10.0 1.1 fusion.30
  11.1 0.9 fusion.28
  12.0 8.0 %all_gather.12 = bf16[24,512]{1,0:T(8,128)(2,1)} all-gather(bf16[24,128]{1,0:T(8,128)(2,1)} %param.19), channel_id=1, replica_groups=mesh['kv'=8,'tp'=4] {'tp'}, dimensions={1}, use_global_device_ids=true | all-gather | bytes 30720 | tf_op jit(solution)/shard_map/all_gather | solution.py:61
  20.0 40.5 %all-reduce = (f32[24]{0:T(128)S(1)}, f32[24,512]{1,0:T(8,128)S(1)}, f32[24,64]{1,0:T(8,128)S(1)}) all-reduce(f32[24]{0:T(128)S(1)} %fusion.26, f32[24,512]{1,0:T(8,128)S(1)} %fusion.30, f32[24,64]{1,0:T(8,128)S(1)} %fusion.28), channel_id=1, replica_groups=mesh['kv'=8,'tp'=4] {'kv','tp'}, use_global_device_ids=true, to_apply=%region_1.0 | all-reduce | flops 13848 | bytes 110784 | tf_op jit(solution)/shard_map/psum | solution.py:64
  60.5 0.0 copy-start.6
  60.5 0.2 multiply_reduce_fusion.5
  60.7 0.1 broadcast_multiply_fusion
  60.8 0.8 fusion.20
  61.6 0.7 subtract_convert_fusion.1
  62.3 0.7 maximum_convert_fusion
  63.0 75.0 %all-reduce.5.cloned.1.call-done = f32[24,1536]{1,0:T(8,128)} async-done(((f32[24,1536]{1,0:T(8,128)}), f32[24,1536]{1,0:T(8,128)}) %all-reduce.5.cloned.1.call-update) | async-done | bytes 147472 | tf_op jit(solution)/shard_map/psum | solution.py:64
  137.9 1.1 multiply_reduce_fusion.1
  139.1 0.0 copy-start.9
  139.1 1.5 fusion.38
  140.6 0.0 copy-done.6
  140.6 0.0 copy-done.9
  140.6 0.1 reshape.98
  140.7 0.7 subtract_convert_fusion
  141.4 1.9 fusion.4
  143.3 0.0 copy-done.4
  143.3 0.3 multiply_reduce_fusion
  143.6 4.6 %fusion.10 = f32[24,4,256]{2,1,0:T(4,128)S(1)} fusion(bf16[24,256,512]{2,1,0:T(8,128)(2,1)} %param.30, bf16[24,4,512]{2,0,1:T(8,128)(2,1)S(1)} %get-tuple-element.23), kind=kOutput, calls=%fused_computation.24 | convolution fusion | flops 25165824 | bytes 6488064 | tf_op jit(solution)/shard_map/bhc,bpc->bhp/dot_general | solution.py:92
  148.2 0.0 copy-done.2
  148.2 0.4 fusion.41
  148.6 0.1 copy.41
  148.7 0.8 fusion.15
  149.4 4.4 %convolution_convert_fusion.2 = bf16[24,4,512]{2,1,0:T(4,128)(2,1)} fusion(bf16[24,256,512]{2,1,0:T(8,128)(2,1)} %param.30, f32[24,4,256]{2,1,0:T(4,128)S(1)} %get-tuple-element.21, f32[24,4]{1,0:T(8,128)S(1)} %get-tuple-element.20), kind=kOutput, calls=%fused_computation.4 | convolution fusion | flops 25264128 | bytes 6488448 | tf_op jit(solution)/shard_map/bhp,bpc->bhc/dot_general | solution.py:98
  153.8 28.4 %all-gather.3 = f32[8,24,4]{1,2,0:T(4,128)S(1)} all-gather(f32[1,24,4]{1,2,0:T(4,128)S(1)} %bitcast.42), channel_id=2, replica_groups=mesh['kv'=8,'tp'=4] {'kv'}, dimensions={0}, use_global_device_ids=true | all-gather | bytes 3456 | tf_op jit(solution)/shard_map/all_gather | solution.py:102
  182.2 0.0 copy-done.5
  182.2 0.2 multiply_reduce_fusion.4
  182.4 0.1 copy.42
  182.5 0.8 copy.45
  183.3 26.1 %all-gather.4 = f32[8,24,4]{1,2,0:T(4,128)S(1)} all-gather(f32[1,24,4]{1,2,0:T(4,128)S(1)} %bitcast.43), channel_id=4, replica_groups=mesh['kv'=8,'tp'=4] {'kv'}, dimensions={0}, use_global_device_ids=true | all-gather | bytes 3456 | tf_op jit(solution)/shard_map/all_gather | solution.py:103
  209.4 0.6 multiply_reduce_fusion.6
  210.0 0.6 fusion.40
  210.6 0.8 copy.43
  211.5 32.5 %all-gather.1 = bf16[192,4,512]{2,1,0:T(4,128)(2,1)S(1)} all-gather(bf16[24,4,512]{2,1,0:T(4,128)(2,1)} %convolution_convert_fusion.2), channel_id=3, replica_groups=mesh['kv'=8,'tp'=4] {'kv'}, dimensions={0}, use_global_device_ids=true | all-gather | bytes 884736 | tf_op jit(solution)/shard_map/all_gather | solution.py:119
  244.0 0.5 fusion
  244.5 0.0 copy-start.7
  244.5 1.4 multiply_reduce_fusion.3
  246.0 0.2 convolution_convert_fusion.6
  246.1 10.3 %psum.68 = bf16[24,512]{1,0:T(8,128)(2,1)S(1)} all-reduce(bf16[24,512]{1,0:T(8,128)(2,1)S(1)} %convolution_convert_fusion.6), channel_id=1, replica_groups=mesh['kv'=8,'tp'=4] {'tp'}, use_global_device_ids=true, to_apply=%region_16.0 | all-reduce | flops 12288 | bytes 49152 | tf_op jit(solution)/shard_map/psum | solution.py:131
  256.4 6.3 %psum.67 = f32[24]{0:T(128)S(1)} all-reduce(f32[24]{0:T(128)S(1)} %get-tuple-element.24), channel_id=1, replica_groups=mesh['kv'=8,'tp'=4] {'tp'}, use_global_device_ids=true, to_apply=%region_15.0 | all-reduce | flops 24 | bytes 192 | tf_op jit(solution)/shard_map/psum | solution.py:128
  262.7 1.1 multiply_reduce_fusion.2
  263.8 1.8 convolution_convert_fusion
  265.6 0.0 copy-done.7
  265.6 1.1 convolution_convert_fusion.1
  266.8 0.0 all-reduce.7.cloned.1.call-update
  266.8 0.0 reduce-scatter.4.cloned.1.call-start
  266.8 18.2 %psum.69 = bf16[24]{0:T(256)(128)(2,1)S(1)} all-reduce(bf16[24]{0:T(256)(128)(2,1)S(1)} %get-tuple-element.10), channel_id=1, replica_groups=mesh['kv'=8,'tp'=4] {'kv'}, use_global_device_ids=true, to_apply=%region_18.0 | all-reduce | flops 24 | bytes 96 | tf_op jit(solution)/shard_map/psum | solution.py:142
  285.0 50.3 %all-reduce.7.cloned.1.call-done = (bf16[24,2816]{1,0:T(8,128)(2,1)}, bf16[24,2816]{1,0:T(8,128)(2,1)}) async-done(((bf16[24,2816]{1,0:T(8,128)(2,1)}, bf16[24,2816]{1,0:T(8,128)(2,1)}), (bf16[24,2816]{1,0:T(8,128)(2,1)}, bf16[24,2816]{1,0:T(8,128)(2,1)})) %all-reduce.7.cloned.1.call-update) | async-done | bytes 270352 | tf_op jit(solution)/shard_map/psum | solution.py:141
  335.3 2.5 convolution_convert_fusion.5
  337.9 0.7 copy.47
  338.6 0.0 reduce-scatter.4.cloned.1.call-update
  338.6 19.1 %reduce-scatter.4.cloned.1.call-done = bf16[128,24]{1,0:T(8,128)(2,1)} async-done(((bf16[512,24]{1,0:T(8,128)(2,1)}), bf16[128,24]{1,0:T(8,128)(2,1)}) %reduce-scatter.4.cloned.1.call-update) | async-done | bytes 6160
  357.7 0.8 copy.48
  358.5 0.6 add_convert_fusion.2
  (17 shorter events, 0.1 us)
Async XLA Ops:
  6.5 257.2 %copy-start = (bf16[512,2816]{1,0:T(8,128)(2,1)S(1)}, bf16[512,2816]{1,0:T(8,128)(2,1)}, u32[]{:S(2)}) copy-start(bf16[512,2816]{1,0:T(8,128)(2,1)} %param.36) | copy-start | bytes 8650756
  6.5 136.8 %copy-start.4 = (bf16[4,128,512]{2,1,0:T(8,128)(2,1)S(1)}, bf16[4,128,512]{2,1,0:T(8,128)(2,1)}, u32[]{:S(2)}) copy-start(bf16[4,128,512]{2,1,0:T(8,128)(2,1)} %param.28) | copy-start | bytes 1572868
  6.5 131.4 %all-reduce.5.cloned.1.call-start = ((), (), s32[]{:S(2)}) async-start(), calls=%async_computation.1 | async-start | bytes 294912 | tf_op jit(solution)/shard_map/psum | solution.py:64
  8.6 326.8 %all-reduce.7.cloned.1.call-start = ((), (), s32[]{:S(2)}) async-start(), calls=%async_computation.3 | async-start | bytes 540672 | tf_op jit(solution)/shard_map/psum | solution.py:141
  60.5 80.1 %copy-start.6 = (f32[24]{0:T(128)}, f32[24]{0:T(128)S(1)}, u32[]{:S(2)}) copy-start(f32[24]{0:T(128)S(1)} %add_rsqrt_fusion.4) | copy-start | bytes 292
  139.1 1.5 copy-start.9
  143.6 4.6 %copy-start.2 = (bf16[24,256,64]{1,2,0:T(8,128)(2,1)S(1)}, bf16[24,256,64]{1,2,0:T(8,128)(2,1)}, u32[]{:S(2)}) copy-start(bf16[24,256,64]{1,2,0:T(8,128)(2,1)} %param.31) | copy-start | bytes 2359300
  149.4 32.8 %copy-start.5 = (f32[24,64]{1,0:T(8,128)S(1)}, f32[24,64]{1,0:T(8,128)}, u32[]{:S(2)}) copy-start(f32[24,64]{1,0:T(8,128)} %maximum_convert_fusion) | copy-start | bytes 18436
  153.8 92.1 %copy-start.3 = (bf16[512,512]{1,0:T(8,128)(2,1)S(1)}, bf16[512,512]{1,0:T(8,128)(2,1)}, u32[]{:S(2)}) copy-start(bf16[512,512]{1,0:T(8,128)(2,1)} %param.33) | copy-start | bytes 1572868
  211.5 34.5 %copy-start.8 = (f32[512]{0:T(512)S(1)}, f32[512]{0:T(512)}, u32[]{:S(2)}) copy-start(f32[512]{0:T(512)} %param.32) | copy-start | bytes 6148
  244.5 21.1 %copy-start.7 = (f32[512]{0:T(512)S(1)}, f32[512]{0:T(512)}, u32[]{:S(2)}) copy-start(f32[512]{0:T(512)} %param.34) | copy-start | bytes 6148
  262.7 2.9 copy-start.1
  266.8 90.9 %reduce-scatter.4.cloned.1.call-start = ((), (), s32[]{:S(2)}) async-start(), calls=%async_computation.2 | async-start | bytes 163840
Sparse Core Ops, SparseCore 0:
  12.9 125.0 all-reduce.4
  266.9 68.3 all-reduce.6
  338.8 18.9 reduce-scatter.3
where the time goes:
time: 367 us; the launch traced here: 366 us
  blocking collectives  170 us (46%)
  waiting for transfers between devices  144 us (39%)
  matrix products  24.1 us (7%)
  between operations  13.2 us (4%)
  other arithmetic  10.1 us (3%)
    psum x1, waiting for transfers between devices, local(): lax.psum((matmul(first_scaled, query_down), matmul(first_scaled, latent_d...  75 us
    psum x1, waiting for transfers between devices, local(): lax.psum(up_part.astype(jnp.bfloat16), 'kv').astype(jnp.float32)  50.3 us
    psum x1, blocking collectives, local(): lax.psum((matmul(first_scaled, query_down), matmul(first_scaled, latent_d...  40.5 us
    all_gather x1, blocking collectives, local(): lax.all_gather(weighted[None], 'kv', axis=0, tiled=True).astype(jnp.float32)  32.5 us
    all_gather x1, blocking collectives, local(): lax.all_gather(maxima[None], 'kv', axis=0, tiled=True)  28.4 us
    all_gather x1, blocking collectives, local(): lax.all_gather(totals[None], 'kv', axis=0, tiled=True)  26.1 us
    unnamed x4, waiting for transfers between devices  19.1 us
    psum x1, blocking collectives, local(): lax.psum(sum_squares(middle_f).astype(jnp.bfloat16), 'kv')  18.2 us
  transfers between devices with their start and end apart: 3, of which 3 were waited for; matrix products, arithmetic and copies ran while one was open for 2% of the time, Pallas kernels for 0%

commit v1 on v0

--- a/solution.py
+++ b/solution.py
@@ -136,9 +136,14 @@
     second_scaled = (middle_f * mixer_gain).astype(jnp.bfloat16)
     gate_part = matmul(second_scaled, gate_weight)
     up_part = matmul(second_scaled, up_weight)
+
+    def list_regions_on_mesh(original, lane_axis):
+        fresh = jnp.sum(lax.all_gather(original, axis_name=lane_axis), axis=0)
+        return fresh
+
     gate_total, up_total, middle_square = (
         lax.psum(gate_part.astype(jnp.bfloat16), "kv").astype(jnp.float32),
-        lax.psum(up_part.astype(jnp.bfloat16), "kv").astype(jnp.float32),
+        list_regions_on_mesh(up_part.astype(jnp.bfloat16), "kv").astype(jnp.float32),
         lax.psum(sum_squares(middle_f).astype(jnp.bfloat16), "kv").astype(jnp.float32),
     )
     second_scale = lax.rsqrt(middle_square / model_width + epsilon)[:, None]

time: 367 us -> 407 us (1.11)
  waiting for transfers between devices: 144 us -> 182 us
    psum x1, waiting for transfers between devices: 50.3 us -> 71.1 us  [local(): lax.psum(gate_part.astype(jnp.bfloat16), 'kv').astype(jnp.float32)]
    all_gather x0 -> x1, waiting for transfers between devices: none -> 16.5 us  [list_regions_on_mesh(): fresh = jnp.sum(lax.all_gather(original, axis_name=lane_axis), axis=0)]
    unnamed x4 -> x5, waiting for transfers between devices: 19.1 us -> 18.9 us
  transfers between devices with their start and end apart: 3 -> 4, of which waited for: 3 -> 4; matrix products, arithmetic and copies ran while one was open for 2% -> 3% of each run, Pallas kernels for 0% -> 0%
where the time goes in v1:
time: 407 us; the launch traced here: 406 us
  waiting for transfers between devices  182 us (45%)
  blocking collectives  170 us (42%)
  matrix products  25.8 us (6%)
  between operations  13.3 us (3%)
  other arithmetic  11.4 us (3%)
    psum x1, waiting for transfers between devices, local(): lax.psum((matmul(first_scaled, query_down), matmul(first_scaled, latent_d...  75 us
    psum x1, waiting for transfers between devices, local(): lax.psum(gate_part.astype(jnp.bfloat16), 'kv').astype(jnp.float32)  71.1 us
    psum x1, blocking collectives, local(): lax.psum((matmul(first_scaled, query_down), matmul(first_scaled, latent_d...  40.4 us
    all_gather x1, blocking collectives, local(): lax.all_gather(weighted[None], 'kv', axis=0, tiled=True).astype(jnp.float32)  32.5 us
    all_gather x1, blocking collectives, local(): lax.all_gather(maxima[None], 'kv', axis=0, tiled=True)  28.4 us
    all_gather x1, blocking collectives, local(): lax.all_gather(totals[None], 'kv', axis=0, tiled=True)  26.1 us
    unnamed x5, waiting for transfers between devices  18.9 us
    psum x1, blocking collectives, local(): lax.psum(sum_squares(middle_f).astype(jnp.bfloat16), 'kv')  18.1 us
  transfers between devices with their start and end apart: 4, of which 4 were waited for; matrix products, arithmetic and copies ran while one was open for 3% of the time, Pallas kernels for 0%

profile of v1, /device:TPU:0, one launch (start us, length us, event | category | flops | bytes accessed | tf_op | source)
XLA Modules:
  0.0 405.7 jit_solution(13791331316202314132)
XLA Ops:
  6.5 0.0 copy-start
  6.5 0.0 all-reduce.4.cloned.1.call-start
  6.5 2.0 fusion.32
  8.5 0.0 all-reduce.4.cloned.1.call-update
  8.6 0.0 all-gather.8.cloned.1.call-start
  8.6 0.8 fusion.26
  9.4 0.6 fusion.35
  10.0 1.1 fusion.30
  11.1 0.9 fusion.28
  12.0 8.0 %all_gather.18 = bf16[24,512]{1,0:T(8,128)(2,1)} all-gather(bf16[24,128]{1,0:T(8,128)(2,1)} %param.19), channel_id=1, replica_groups=mesh['kv'=8,'tp'=4] {'tp'}, dimensions={1}, use_global_device_ids=true | all-gather | bytes 30720 | tf_op jit(solution)/shard_map/all_gather | solution.py:61
  20.0 40.4 %all-reduce = (f32[24]{0:T(128)S(1)}, f32[24,512]{1,0:T(8,128)S(1)}, f32[24,64]{1,0:T(8,128)S(1)}) all-reduce(f32[24]{0:T(128)S(1)} %fusion.26, f32[24,512]{1,0:T(8,128)S(1)} %fusion.30, f32[24,64]{1,0:T(8,128)S(1)} %fusion.28), channel_id=1, replica_groups=mesh['kv'=8,'tp'=4] {'kv','tp'}, use_global_device_ids=true, to_apply=%region_1.0 | all-reduce | flops 13848 | bytes 110784 | tf_op jit(solution)/shard_map/psum | solution.py:64
  60.5 0.2 multiply_reduce_fusion.5
  60.7 0.1 broadcast_multiply_fusion
  60.8 0.8 fusion.20
  61.5 0.7 subtract_convert_fusion.1
  62.3 0.7 maximum_convert_fusion
  62.9 75.0 %all-reduce.4.cloned.1.call-done = f32[24,1536]{1,0:T(8,128)} async-done(((f32[24,1536]{1,0:T(8,128)}), f32[24,1536]{1,0:T(8,128)}) %all-reduce.4.cloned.1.call-update) | async-done | bytes 147472 | tf_op jit(solution)/shard_map/psum | solution.py:64
  137.9 1.1 multiply_reduce_fusion.1
  139.1 0.0 copy-start.8
  139.1 1.5 fusion.38
  140.6 0.0 copy-done.5
  140.6 0.1 reshape.98
  140.7 0.7 subtract_convert_fusion
  141.4 1.9 fusion.4
  143.3 0.0 copy-done.3
  143.3 0.3 multiply_reduce_fusion
  143.6 4.6 %fusion.10 = f32[24,4,256]{2,1,0:T(4,128)S(1)} fusion(bf16[24,256,512]{2,1,0:T(8,128)(2,1)} %param.30, bf16[24,4,512]{2,0,1:T(8,128)(2,1)S(1)} %get-tuple-element.21), kind=kOutput, calls=%fused_computation.24 | convolution fusion | flops 25165824 | bytes 6488064 | tf_op jit(solution)/shard_map/bhc,bpc->bhp/dot_general | solution.py:92
  148.2 0.4 fusion.41
  148.6 0.1 copy.41
  148.7 0.8 fusion.15
  149.4 4.4 %convolution_convert_fusion.2 = bf16[24,4,512]{2,1,0:T(4,128)(2,1)} fusion(bf16[24,256,512]{2,1,0:T(8,128)(2,1)} %param.30, f32[24,4,256]{2,1,0:T(4,128)S(1)} %get-tuple-element.19, f32[24,4]{1,0:T(8,128)S(1)} %get-tuple-element.18), kind=kOutput, calls=%fused_computation.4 | convolution fusion | flops 25264128 | bytes 6488448 | tf_op jit(solution)/shard_map/bhp,bpc->bhc/dot_general | solution.py:98
  153.8 28.4 %all-gather.4 = f32[8,24,4]{1,2,0:T(4,128)S(1)} all-gather(f32[1,24,4]{1,2,0:T(4,128)S(1)} %bitcast.44), channel_id=2, replica_groups=mesh['kv'=8,'tp'=4] {'kv'}, dimensions={0}, use_global_device_ids=true | all-gather | bytes 3456 | tf_op jit(solution)/shard_map/all_gather | solution.py:102
  182.2 0.2 multiply_reduce_fusion.4
  182.4 0.1 copy.42
  182.5 0.8 copy.45
  183.3 26.1 %all-gather.5 = f32[8,24,4]{1,2,0:T(4,128)S(1)} all-gather(f32[1,24,4]{1,2,0:T(4,128)S(1)} %bitcast.45), channel_id=4, replica_groups=mesh['kv'=8,'tp'=4] {'kv'}, dimensions={0}, use_global_device_ids=true | all-gather | bytes 3456 | tf_op jit(solution)/shard_map/all_gather | solution.py:103
  209.4 0.6 multiply_reduce_fusion.6
  210.0 0.6 fusion.40
  210.6 0.8 copy.43
  211.5 32.5 %all-gather.1 = bf16[192,4,512]{2,1,0:T(4,128)(2,1)S(1)} all-gather(bf16[24,4,512]{2,1,0:T(4,128)(2,1)} %convolution_convert_fusion.2), channel_id=3, replica_groups=mesh['kv'=8,'tp'=4] {'kv'}, dimensions={0}, use_global_device_ids=true | all-gather | bytes 884736 | tf_op jit(solution)/shard_map/all_gather | solution.py:119
  244.0 0.5 fusion
  244.5 0.0 copy-start.6
  244.5 1.4 multiply_reduce_fusion.3
  246.0 0.2 convolution_convert_fusion.6
  246.1 10.3 %psum.61 = bf16[24,512]{1,0:T(8,128)(2,1)S(1)} all-reduce(bf16[24,512]{1,0:T(8,128)(2,1)S(1)} %convolution_convert_fusion.6), channel_id=1, replica_groups=mesh['kv'=8,'tp'=4] {'tp'}, use_global_device_ids=true, to_apply=%region_16.0 | all-reduce | flops 12288 | bytes 49152 | tf_op jit(solution)/shard_map/psum | solution.py:131
  256.4 6.3 %psum.60 = f32[24]{0:T(128)S(1)} all-reduce(f32[24]{0:T(128)S(1)} %get-tuple-element.22), channel_id=1, replica_groups=mesh['kv'=8,'tp'=4] {'tp'}, use_global_device_ids=true, to_apply=%region_15.0 | all-reduce | flops 24 | bytes 192 | tf_op jit(solution)/shard_map/psum | solution.py:128
  262.7 0.9 multiply_reduce_fusion.2
  263.6 1.8 convolution_convert_fusion
  265.5 0.0 all-gather.8.cloned.1.call-update
  265.5 0.0 all-reduce.6.cloned.1.call-start
  265.5 18.1 %psum.62 = bf16[24]{0:T(256)(128)(2,1)S(1)} all-reduce(bf16[24]{0:T(256)(128)(2,1)S(1)} %get-tuple-element.8), channel_id=1, replica_groups=mesh['kv'=8,'tp'=4] {'kv'}, use_global_device_ids=true, to_apply=%region_18.0 | all-reduce | flops 24 | bytes 96 | tf_op jit(solution)/shard_map/psum | solution.py:147
  283.6 0.0 copy-done.6
  283.6 3.0 convolution_convert_fusion.1
  286.6 0.0 all-reduce.6.cloned.1.call-update
  286.6 0.0 reduce-scatter.4.cloned.1.call-start
  286.7 16.5 %all-gather.8.cloned.1.call-done = bf16[192,2816]{1,0:T(8,128)(2,1)} async-done(((bf16[24,2816]{1,0:T(8,128)(2,1)}), bf16[192,2816]{1,0:T(8,128)(2,1)}) %all-gather.8.cloned.1.call-update) | async-done | bytes 1081360 | tf_op jit(solution)/shard_map/all_gather | solution.py:141
  303.2 1.4 reduce_sum.112
  304.6 71.1 %all-reduce.6.cloned.1.call-done = bf16[24,2816]{1,0:T(8,128)(2,1)} async-done(((bf16[24,2816]{1,0:T(8,128)(2,1)}), bf16[24,2816]{1,0:T(8,128)(2,1)}) %all-reduce.6.cloned.1.call-update) | async-done | bytes 135184 | tf_op jit(solution)/shard_map/psum | solution.py:145
  375.7 2.5 convolution_convert_fusion.5
  378.1 0.7 copy.47
  378.9 0.0 reduce-scatter.4.cloned.1.call-update
  378.9 18.9 %reduce-scatter.4.cloned.1.call-done = bf16[128,24]{1,0:T(8,128)(2,1)} async-done(((bf16[512,24]{1,0:T(8,128)(2,1)}), bf16[128,24]{1,0:T(8,128)(2,1)}) %reduce-scatter.4.cloned.1.call-update) | async-done | bytes 6160
  397.8 0.8 copy.48
  398.6 0.6 add_convert_fusion.2
  (19 shorter events, 0.1 us)
Async XLA Ops:
  6.5 257.1 %copy-start = (bf16[512,2816]{1,0:T(8,128)(2,1)S(1)}, bf16[512,2816]{1,0:T(8,128)(2,1)}, u32[]{:S(2)}) copy-start(bf16[512,2816]{1,0:T(8,128)(2,1)} %param.36) | copy-start | bytes 8650756
  6.5 136.8 %copy-start.3 = (bf16[4,128,512]{2,1,0:T(8,128)(2,1)S(1)}, bf16[4,128,512]{2,1,0:T(8,128)(2,1)}, u32[]{:S(2)}) copy-start(bf16[4,128,512]{2,1,0:T(8,128)(2,1)} %param.28) | copy-start | bytes 1572868
  6.5 131.4 %all-reduce.4.cloned.1.call-start = ((), (), s32[]{:S(2)}) async-start(), calls=%async_computation.1 | async-start | bytes 294912 | tf_op jit(solution)/shard_map/psum | solution.py:64
  8.6 294.6 %all-gather.8.cloned.1.call-start = ((), (), s32[]{:S(2)}) async-start(), calls=%async_computation.3 | async-start | bytes 1216512 | tf_op jit(solution)/shard_map/all_gather | solution.py:141
  60.5 80.1 %copy-start.5 = (f32[24]{0:T(128)}, f32[24]{0:T(128)S(1)}, u32[]{:S(2)}) copy-start(f32[24]{0:T(128)S(1)} %add_rsqrt_fusion.4) | copy-start | bytes 292
  139.1 1.5 copy-start.8
  143.6 4.6 %copy-start.1 = (bf16[24,256,64]{1,2,0:T(8,128)(2,1)S(1)}, bf16[24,256,64]{1,2,0:T(8,128)(2,1)}, u32[]{:S(2)}) copy-start(bf16[24,256,64]{1,2,0:T(8,128)(2,1)} %param.31) | copy-start | bytes 2359300
  149.4 32.8 %copy-start.4 = (f32[24,64]{1,0:T(8,128)S(1)}, f32[24,64]{1,0:T(8,128)}, u32[]{:S(2)}) copy-start(f32[24,64]{1,0:T(8,128)} %maximum_convert_fusion) | copy-start | bytes 18436
  153.8 92.1 %copy-start.2 = (bf16[512,512]{1,0:T(8,128)(2,1)S(1)}, bf16[512,512]{1,0:T(8,128)(2,1)}, u32[]{:S(2)}) copy-start(bf16[512,512]{1,0:T(8,128)(2,1)} %param.33) | copy-start | bytes 1572868
  211.5 34.5 %copy-start.7 = (f32[512]{0:T(512)S(1)}, f32[512]{0:T(512)}, u32[]{:S(2)}) copy-start(f32[512]{0:T(512)} %param.32) | copy-start | bytes 6148
  244.5 39.1 %copy-start.6 = (f32[512]{0:T(512)S(1)}, f32[512]{0:T(512)}, u32[]{:S(2)}) copy-start(f32[512]{0:T(512)} %param.34) | copy-start | bytes 6148
  265.5 110.2 %all-reduce.6.cloned.1.call-start = ((), (), s32[]{:S(2)}) async-start(), calls=%async_computation.2 | async-start | bytes 270336 | tf_op jit(solution)/shard_map/psum | solution.py:145
  286.6 111.2 %reduce-scatter.4.cloned.1.call-start = ((), (), s32[]{:S(2)}) async-start(), calls=%async_computation.4 | async-start | bytes 163840
Sparse Core Ops, SparseCore 0:
  12.9 125.0 all-reduce.3
  265.6 37.5 all-gather.7
  306.5 69.0 all-reduce.5
  379.0 18.7 reduce-scatter.3
